TPU v7x, 32 devices: a whole 2x2x4 slice. The times are simulated.
32 devices in a mesh: sp: 8 (over z, y), dp: 4 (over x, core).
Axes of the slice: x: 2, y: 2, z: 4, core: 2. Of those that a mesh axis runs over, the one named last changes fastest.
Arguments:
- residual: bfloat16 [4, 1024, 2048], P('dp', 'sp'), may hold values from -6 to 6
- query: bfloat16 [4, 1024, 1536], P('dp', 'sp'), may hold values from -64 to 64
- latent: bfloat16 [4, 1024, 256], P('dp', 'sp'), may hold values from -6 to 6
- rope_key: bfloat16 [4, 1024, 32], P('dp', 'sp'), may hold values from -64 to 64
- latent_gain: float32 [256], replicated, may hold values from 0.1 to 1.9
- query_gain: float32 [96], replicated, may hold values from 0.7 to 5.6
- key_gain: float32 [96], replicated, may hold values from 0.7 to 5.6
- key_weight: bfloat16 [256, 1024], replicated, may hold values from -0.375 to 0.375
- value_weight: bfloat16 [256, 1024], replicated, may hold values from -0.375 to 0.375
- mix_gain: float32 [1024], replicated, may hold values from 0.1 to 1.9
- out_weight: bfloat16 [1024, 2048], replicated, may hold values from -0.1875 to 0.1875
- ffn_gain: float32 [2048], replicated, may hold values from 0.1 to 1.9
- expert_choice: int32 [4, 1024, 2], P('dp', 'sp'), may hold values from 0 to 31, as said below
- group_prob: float32 [4, 1024], P('dp', 'sp'), may hold values from 0.25 to 1
- expert_prob: float32 [4, 1024, 2], P('dp', 'sp'), may hold values from 0.05 to 1
- gate_weight: bfloat16 [32, 2048, 512], P(('sp', 'dp')), may hold values from -0.125 to 0.125
- up_weight: bfloat16 [32, 2048, 512], P(('sp', 'dp')), may hold values from -0.125 to 0.125
- down_weight: bfloat16 [32, 512, 2048], P(('sp', 'dp')), may hold values from -0.25 to 0.25
Outputs:
- layer_out: bfloat16 [4, 1024, 2048], P('dp', 'sp')
Inputs may be any that keep to these rules, and one draw needn't show every extreme that they name: `expert_choice`: A token's two experts differ and lie in one group of 8 consecutive expert numbers. In each aligned block of 128 tokens (the tokens of one device) no expert is named more than 16 times, and every expert of one group is named exactly 16 times in every block.
All inputs are finite; a program needn't handle non-finite values.
Results may differ from a plain program's by a relative error of at most 0.012.
The roundings to bfloat16 on the way count: a program that leaves them out, or rounds other values in their place, can miss the bound.
Values may be sent and summed in bfloat16 or wider, within the bound.
A program may use at most 64 MiB of HBM per device.

v0:
```python
import jax
import jax.numpy as jnp
from jax import lax
from jax.sharding import PartitionSpec as P

GROUPS = 4
SPAN = 64


eps = 1e-06


def rms_scale(vector, gains):
    return vector * lax.rsqrt(jnp.mean(vector * vector, axis=-1, keepdims=True) + eps) * gains


def rotate(vector, phases):
    half_width = vector.shape[-1] // 2
    lower_half = vector[..., :half_width]
    upper_half = vector[..., half_width:]
    cos_table = jnp.cos(phases)
    sin_table = jnp.sin(phases)
    return jnp.concatenate(
        [
            lower_half * cos_table - upper_half * sin_table,
            upper_half * cos_table + lower_half * sin_table,
        ],
        axis=-1,
    )


def angles(offset, span_count, rope_width):
    position = (offset + jnp.arange(span_count, dtype=jnp.int32)).astype(jnp.float32)
    frequency = 10000.0 ** (-2.0 * jnp.arange(rope_width // 2, dtype=jnp.float32) / rope_width)
    return position[:, None] * frequency[None, :]


def head_vectors(nope_part, rope_part, gains, phases):
    normed_all = rms_scale(jnp.concatenate([nope_part, rope_part], axis=-1), gains)
    split_at = nope_part.shape[-1]
    turned = rotate(normed_all[..., split_at:], phases[:, None, :])
    return jnp.concatenate([normed_all[..., :split_at], turned], axis=-1).astype(jnp.bfloat16)


def attend(queries_head, keys_head, values_head):
    length = queries_head.shape[0]
    blocks_count = max(4, length // 1024)
    block_rows = length // blocks_count
    score_scale = queries_head.shape[-1] ** (-0.5)
    pieces = []
    for block_index in range(blocks_count):
        first_row = block_index * block_rows
        last_row = first_row + block_rows
        scores = (
            jnp.einsum(
                "qhd,khd->hqk",
                queries_head[first_row:last_row],
                keys_head[:last_row],
                preferred_element_type=jnp.float32,
            )
            * score_scale
        )
        query_pos = first_row + jnp.arange(block_rows, dtype=jnp.int32)
        key_pos = jnp.arange(last_row, dtype=jnp.int32)
        allowed = key_pos[None, :] // SPAN <= query_pos[:, None] // SPAN
        scores = jnp.where(allowed[None], scores, -1e30)
        row_top = jnp.max(scores, axis=-1, keepdims=True)
        raised = jnp.exp(scores - row_top)
        row_sum = jnp.sum(raised, axis=-1)
        summed = jnp.einsum(
            "hqk,khd->qhd",
            raised.astype(jnp.bfloat16),
            values_head[:last_row],
            preferred_element_type=jnp.float32,
        )
        pieces.append((summed / row_sum.T[:, :, None]).astype(jnp.bfloat16))
    return jnp.concatenate(pieces, axis=0)


def per_device(
    residual,
    query,
    latent,
    rope_key,
    latent_gain,
    query_gain,
    key_gain,
    key_weight,
    value_weight,
    mix_gain,
    out_weight,
    ffn_gain,
    expert_choice,
    group_prob,
    expert_prob,
    gate_weight,
    up_weight,
    down_weight,
):
    tok_rows = residual.shape[1]
    model_width = residual.shape[2]
    rope_width = rope_key.shape[2]
    qk_width = query_gain.shape[0]
    nope_width = qk_width - rope_width
    head_count = query.shape[2] // qk_width
    value_width = value_weight.shape[1] // head_count
    seq_devices = lax.axis_size("sp")
    offset = lax.axis_index("sp") * tok_rows
    own_phases = angles(offset, tok_rows, rope_width)
    raw_query = query[0].astype(jnp.float32).reshape(tok_rows, head_count, qk_width)
    queries_tok = head_vectors(
        raw_query[..., :nope_width], raw_query[..., nope_width:], query_gain, own_phases
    )
    normed_latent = rms_scale(latent[0].astype(jnp.float32), latent_gain).astype(jnp.bfloat16)
    key_part = jnp.dot(normed_latent, key_weight, preferred_element_type=jnp.float32).astype(
        jnp.bfloat16
    )
    values_tok = jnp.dot(normed_latent, value_weight, preferred_element_type=jnp.float32).astype(
        jnp.bfloat16
    )
    values_tok = values_tok.reshape(tok_rows, head_count, value_width)
    shared_rope = jnp.broadcast_to(
        rope_key[0].astype(jnp.float32)[:, None, :], (tok_rows, head_count, rope_width)
    )
    keys_tok = head_vectors(
        key_part.astype(jnp.float32).reshape(tok_rows, head_count, nope_width),
        shared_rope,
        key_gain,
        own_phases,
    )
    queries_head, keys_head, values_head = (
        lax.all_to_all(queries_tok, "sp", split_axis=1, concat_axis=0, tiled=True),
        lax.all_to_all(keys_tok, "sp", split_axis=1, concat_axis=0, tiled=True),
        lax.all_to_all(values_tok, "sp", split_axis=1, concat_axis=0, tiled=True),
    )
    head_out = attend(queries_head, keys_head, values_head)
    token_out = lax.all_to_all(head_out, "sp", split_axis=0, concat_axis=1, tiled=True).reshape(
        tok_rows, head_count * value_width
    )
    mixed_in = rms_scale(token_out.astype(jnp.float32), mix_gain).astype(jnp.bfloat16)
    stream = residual[0].astype(jnp.float32) + jnp.dot(
        mixed_in, out_weight, preferred_element_type=jnp.float32
    )
    normed = rms_scale(stream, ffn_gain).astype(jnp.bfloat16)
    expert_total = seq_devices * lax.axis_size("dp")
    capacity = tok_rows * GROUPS // expert_total
    picked = expert_choice[0].reshape(-1)
    one_hot = (picked[:, None] == jnp.arange(expert_total, dtype=jnp.int32)[None, :]).astype(
        jnp.int32
    )
    earlier = jnp.cumsum(one_hot, axis=0) - one_hot
    slot_rank = jnp.sum(earlier * one_hot, axis=1)
    target = picked * capacity + slot_rank
    source_row = jnp.arange(picked.shape[0], dtype=jnp.int32) // expert_choice.shape[2]
    slot_token = (
        jnp.full((expert_total * capacity,), tok_rows, jnp.int32).at[target].set(source_row)
    )
    padded = jnp.concatenate([normed, jnp.zeros((1, model_width), jnp.bfloat16)], axis=0)
    outgoing = padded[slot_token].reshape(expert_total, capacity, model_width)
    arrived = lax.all_to_all(outgoing, ("sp", "dp"), split_axis=0, concat_axis=0, tiled=True)
    flat_rows = arrived.reshape(-1, model_width)
    gate_act = jnp.dot(flat_rows, gate_weight[0], preferred_element_type=jnp.float32)
    upward = jnp.dot(flat_rows, up_weight[0], preferred_element_type=jnp.float32)
    hidden = (jax.nn.silu(gate_act) * upward).astype(jnp.bfloat16)
    returned = lax.all_to_all(
        jnp.dot(hidden, down_weight[0], preferred_element_type=jnp.float32)
        .astype(jnp.bfloat16)
        .reshape(arrived.shape),
        ("sp", "dp"),
        split_axis=0,
        concat_axis=0,
        tiled=True,
    )
    gathered_rows = returned.reshape(-1, model_width)[target].reshape(
        tok_rows, expert_choice.shape[2], model_width
    )
    expert_share = expert_prob[0]
    route_weight = (
        group_prob[0][:, None] * expert_share / jnp.sum(expert_share, axis=-1, keepdims=True)
    )
    routed_sum = route_weight[:, 0:1] * gathered_rows[:, 0].astype(jnp.float32) + route_weight[
        :, 1:2
    ] * gathered_rows[:, 1].astype(jnp.float32)
    return (stream + routed_sum).astype(jnp.bfloat16)[None]


def solution(mesh):
    return jax.shard_map(
        per_device,
        mesh=mesh,
        in_specs=(
            P("dp", "sp", None),
            P("dp", "sp", None),
            P("dp", "sp", None),
            P("dp", "sp", None),
            P(),
            P(),
            P(),
            P(),
            P(),
            P(),
            P(),
            P(),
            P("dp", "sp", None),
            P("dp", "sp"),
            P("dp", "sp", None),
            P(("sp", "dp"), None, None),
            P(("sp", "dp"), None, None),
            P(("sp", "dp"), None, None),
        ),
        out_specs=P("dp", "sp", None),
        check_vma=False,
    )
```

profile of v0, /device:TPU:0, one launch (start us, length us, event | category | flops | bytes accessed | tf_op | source)
XLA Modules:
  0.0 222.8 jit_solution(3537929885932184085)
XLA Ops:
  0.0 1.1 fusion.52
  1.1 1.4 convolution_convert_fusion.2
  2.5 0.8 copy.84
  3.3 7.3 %all-to-all-start = ((bf16[128,16,64]{0,2,1:T(8,128)(2,1)}), bf16[128,16,64]{0,2,1:T(8,128)(2,1)S(1)}, u32[]{:S(2)}, u32[]{:S(2)}) async-start(bf16[128,16,64]{0,2,1:T(8,128)(2,1)} %bitcast.3), calls=%async_computation | async-start | bytes 524288 | tf_op jit(solution)/shard_map/all_to_all | solution.py:134
  11.2 0.6 and_select_fusion.4
  12.3 1.4 fusion.18
  14.0 1.2 copy.86
  15.3 0.6 add_convert_fusion.2
  15.9 1.4 copy.95
  17.3 1.6 eq.29
  18.9 1.3 fusion.58
  20.2 1.9 reduce-window.6
  22.0 1.5 slice_reduce_fusion
  23.6 0.8 multiply_cosine_fusion
  24.4 0.9 fusion.37
  25.4 0.8 copy-done.3
  26.4 0.8 pad_maximum_fusion.2
  27.1 6.0 %all-to-all-start.2 = ((bf16[128,16,96]{0,2,1:T(8,128)(2,1)}), bf16[128,16,96]{0,2,1:T(8,128)(2,1)S(1)}, u32[]{:S(2)}, u32[]{:S(2)}) async-start(bf16[128,16,96]{0,2,1:T(8,128)(2,1)} %pad_maximum_fusion.2), calls=%async_computation.2 | async-start | bytes 786432 | tf_op jit(solution)/shard_map/all_to_all | solution.py:133
  33.2 1.1 slice.176
  34.8 0.8 pad_maximum_fusion.1
  35.6 0.7 broadcast_compare_fusion.3
  36.3 7.9 %all-to-all-done.2 = bf16[128,16,96]{0,2,1:T(8,128)(2,1)S(1)} async-done(((bf16[128,16,96]{0,2,1:T(8,128)(2,1)}), bf16[128,16,96]{0,2,1:T(8,128)(2,1)S(1)}, u32[]{:S(2)}, u32[]{:S(2)}) %all-to-all-start.2) | async-done | bytes 393248 | tf_op jit(solution)/shard_map/all_to_all | solution.py:133
  44.3 3.7 %all-to-all-start.1 = ((bf16[128,16,96]{0,2,1:T(8,128)(2,1)}), bf16[128,16,96]{0,2,1:T(8,128)(2,1)S(1)}, u32[]{:S(2)}, u32[]{:S(2)}) async-start(bf16[128,16,96]{0,2,1:T(8,128)(2,1)} %pad_maximum_fusion.1), calls=%async_computation.1 | async-start | bytes 786432 | tf_op jit(solution)/shard_map/all_to_all | solution.py:132
  48.0 0.8 broadcast_compare_fusion.2
  48.8 0.9 broadcast_compare_fusion.1
  49.8 1.1 copy.117
  51.0 0.7 slice.143
  51.7 0.8 all_to_all.59
  52.5 1.5 slice.108
  54.0 0.7 slice.120
  54.7 0.9 slice.126
  55.8 0.7 slice.151
  56.5 0.7 slice.154
  57.4 1.6 slice.118
  59.7 0.9 fusion.78
  60.7 0.7 slice.113
  61.4 1.7 slice.124
  63.0 0.7 slice.122
  64.1 0.7 slice.128
  64.8 1.0 slice.132
  65.8 1.3 fusion.81
  67.2 1.1 fusion.24
  69.6 0.6 fusion.79
  70.6 0.6 fusion.26
  71.2 0.7 fusion.5
  71.9 0.7 fusion.6
  72.5 0.7 fusion.23
  73.7 1.1 reshape.673
  74.7 5.6 %all-to-all-start.3 = ((bf16[8,2,8192]{2,1,0:T(2,128)(2,1)}), bf16[8,2,8192]{2,1,0:T(2,128)(2,1)S(1)}, u32[]{:S(2)}, u32[]{:S(2)}) async-start(bf16[8,2,8192]{2,1,0:T(2,128)(2,1)} %reshape.673), calls=%async_computation.3 | async-start | bytes 524288 | tf_op jit(solution)/shard_map/all_to_all | solution.py:137
  80.3 1.6 scatter_custom_fusion
  81.9 6.7 %all-to-all-done.3 = bf16[8,2,8192]{2,1,0:T(2,128)(2,1)S(1)} async-done(((bf16[8,2,8192]{2,1,0:T(2,128)(2,1)}), bf16[8,2,8192]{2,1,0:T(2,128)(2,1)S(1)}, u32[]{:S(2)}, u32[]{:S(2)}) %all-to-all-start.3) | async-done | bytes 262176 | tf_op jit(solution)/shard_map/all_to_all | solution.py:137
  90.4 3.0 %multiply_reduce_fusion = (f32[128]{0:T(128)S(1)}, f32[128,2048]{1,0:T(8,128)S(1)}) fusion(bf16[128,1024]{0,1:T(8,128)(2,1)S(1)} %fusion.45, bf16[1024,2048]{1,0:T(8,128)(2,1)} %param.28, bf16[1,128,2048]{2,1,0:T(8,128)(2,1)S(1)} %copy-done.10), kind=kOutput, calls=%fused_computation.46 | convolution fusion | flops 537919360 | bytes 6029824 | tf_op jit(solution)/shard_map/dot_general | solution.py:141
  93.4 1.0 copy-done.1
  94.6 3.3 %gather_fusion = bf16[512,2048]{1,0:T(8,128)(2,1)} fusion(bf16[129,2048]{1,0:T(8,128)(2,1)S(1)} %concatenate.22, s32[1024]{0:T(1024)S(1)} %pad_clamp_fusion.1), kind=kCustom, calls=%fused_computation | custom fusion | bytes 4196352 | tf_op jit(solution)/shard_map/gather | solution.py:159
  98.0 52.1 %all_to_all.70 = bf16[32,16,2048]{2,1,0:T(8,128)(2,1)S(1)} all-to-all(bf16[32,16,2048]{2,1,0:T(8,128)(2,1)} %bitcast.181), channel_id=1, replica_groups=mesh['sp'=8,'dp'=4] {'sp','dp'}, dimensions={0} | all-to-all | bytes 4194304 | tf_op jit(solution)/shard_map/all_to_all | solution.py:160
  150.1 1.3 copy-done.4
  151.4 2.3 %fusion.3 = f32[512,512]{1,0:T(8,128)} fusion(bf16[512,2048]{1,0:T(8,128)(2,1)S(1)} %bitcast.195, bf16[1,2048,512]{2,1,0:T(8,128)(2,1)S(1)} %copy-done.26), kind=kOutput, calls=%fused_computation.8 | convolution fusion | flops 1073741824 | bytes 5242880 | tf_op jit(solution)/shard_map/dot_general | solution.py:162
  153.7 6.3 %convolution_convert_fusion = bf16[512,2048]{1,0:T(8,128)(2,1)} fusion(bf16[1,512,2048]{2,1,0:T(8,128)(2,1)S(1)} %copy-done, bf16[512,2048]{1,0:T(8,128)(2,1)} %bitcast.196, bf16[1,2048,512]{2,1,0:T(8,128)(2,1)} %param.34, f32[512,512]{1,0:T(8,128)} %fusion.3), kind=kOutput, calls=%fused_computation.3 | convolution fusion | flops 2150105088 | bytes 9437184 | tf_op jit(solution)/shard_map/dot_general | solution.py:166
  159.9 3.8 %all-to-all-start.5 = ((bf16[32,16,2048]{2,1,0:T(8,128)(2,1)}), bf16[32,16,2048]{2,1,0:T(8,128)(2,1)}, u32[]{:S(2)}, u32[]{:S(2)}) async-start(bf16[32,16,2048]{2,1,0:T(8,128)(2,1)} %bitcast.194), calls=%async_computation.5 | async-start | bytes 4194304 | tf_op jit(solution)/shard_map/all_to_all | solution.py:165
  163.8 48.6 %all-to-all-done.5 = bf16[32,16,2048]{2,1,0:T(8,128)(2,1)} async-done(((bf16[32,16,2048]{2,1,0:T(8,128)(2,1)}), bf16[32,16,2048]{2,1,0:T(8,128)(2,1)}, u32[]{:S(2)}, u32[]{:S(2)}) %all-to-all-start.5) | async-done | bytes 2097184 | tf_op jit(solution)/shard_map/all_to_all | solution.py:165
  212.5 5.2 %gather_fusion.1 = bf16[256,2048]{1,0:T(8,128)(2,1)} fusion(bf16[512,2048]{1,0:T(8,128)(2,1)} %bitcast.37, s32[1024]{0:T(1024)S(1)} %pad_clamp_fusion), kind=kCustom, calls=%fused_computation.1 | custom fusion | bytes 2098176 | tf_op jit(solution)/shard_map/gather | solution.py:174
  217.7 1.7 reshape.633
  219.4 1.5 fusion.77
  220.9 1.9 fusion.43
  (110 shorter events, 8.1 us)
Async XLA Ops:
  0.0 153.7 %copy-start = (bf16[1,512,2048]{2,1,0:T(8,128)(2,1)S(1)}, bf16[1,512,2048]{2,1,0:T(8,128)(2,1)}, u32[]{:S(2)}) copy-start(bf16[1,512,2048]{2,1,0:T(8,128)(2,1)} %param.35) | copy-start | bytes 6291460
  0.0 13.9 %copy-start.18 = (bf16[1,128,32]{1,2,0:T(8,128)(2,1)S(1)}, bf16[1,128,32]{1,2,0:T(8,128)(2,1)}, u32[]{:S(2)}) copy-start(bf16[1,128,32]{1,2,0:T(8,128)(2,1)} %param.21) | copy-start | bytes 24580
  3.3 23.8 %all-to-all-start = ((bf16[128,16,64]{0,2,1:T(8,128)(2,1)}), bf16[128,16,64]{0,2,1:T(8,128)(2,1)S(1)}, u32[]{:S(2)}, u32[]{:S(2)}) async-start(bf16[128,16,64]{0,2,1:T(8,128)(2,1)} %bitcast.3), calls=%async_computation | async-start | bytes 524288 | tf_op jit(solution)/shard_map/all_to_all | solution.py:134
  24.3 2.8 %copy-start.20 = (s32[1,128,2]{1,2,0:T(2,128)S(1)}, s32[1,128,2]{1,2,0:T(2,128)}, u32[]{:S(2)}) copy-start(s32[1,128,2]{1,2,0:T(2,128)} %param.30) | copy-start | bytes 3076
  25.3 0.9 copy-start.3
  25.3 8.9 %copy-start.9 = (s32[1,128,2]{2,1,0:T(8,128)S(1)}, s32[1,128,2]{2,1,0:T(8,128)}, u32[]{:S(2)}) copy-start(s32[1,128,2]{2,1,0:T(8,128)} %copy.95) | copy-start | bytes 3076
  25.3 9.1 %copy-start.22 = (s32[32,2]{0,1:T(2,128)S(1)}, s32[32,2]{0,1:T(2,128)}, u32[]{:S(2)}) copy-start(s32[32,2]{0,1:T(2,128)} %slice_reduce_fusion) | copy-start | bytes 772
  25.3 9.4 %copy-start.15 = (s32[32,2,128]{2,0,1:T(8,128)S(1)}, s32[32,2,128]{2,0,1:T(8,128)}, u32[]{:S(2)}) copy-start(s32[32,2,128]{2,0,1:T(8,128)} %reduce-window.6) | copy-start | bytes 98308
  26.2 9.4 %copy-start.21 = (s32[256]{0:T(256)S(1)}, s32[256]{0:T(256)}, u32[]{:S(2)}) copy-start(s32[256]{0:T(256)} %and_select_fusion.4) | copy-start | bytes 3076
  26.3 21.6 %copy-start.24 = (s32[256]{0:T(256)S(1)}, s32[256]{0:T(256)}, u32[]{:S(2)}) copy-start(s32[256]{0:T(256)} %and_select_fusion.3) | copy-start | bytes 3076
  27.1 17.1 %copy-start.5 = (bf16[128,16,64]{0,2,1:T(8,128)(2,1)}, bf16[128,16,64]{0,2,1:T(8,128)(2,1)S(1)}, u32[]{:S(2)}) copy-start(bf16[128,16,64]{0,2,1:T(8,128)(2,1)S(1)} %all-to-all-done) | copy-start | bytes 786436
  27.1 17.1 %all-to-all-start.2 = ((bf16[128,16,96]{0,2,1:T(8,128)(2,1)}), bf16[128,16,96]{0,2,1:T(8,128)(2,1)S(1)}, u32[]{:S(2)}, u32[]{:S(2)}) async-start(bf16[128,16,96]{0,2,1:T(8,128)(2,1)} %pad_maximum_fusion.2), calls=%async_computation.2 | async-start | bytes 786432 | tf_op jit(solution)/shard_map/all_to_all | solution.py:133
  44.3 15.2 %all-to-all-start.1 = ((bf16[128,16,96]{0,2,1:T(8,128)(2,1)}), bf16[128,16,96]{0,2,1:T(8,128)(2,1)S(1)}, u32[]{:S(2)}, u32[]{:S(2)}) async-start(bf16[128,16,96]{0,2,1:T(8,128)(2,1)} %pad_maximum_fusion.1), calls=%async_computation.1 | async-start | bytes 786432 | tf_op jit(solution)/shard_map/all_to_all | solution.py:132
  64.1 4.2 %copy-start.8 = (bf16[512,2,96]{0,2,1:T(8,128)(2,1)S(1)}, bf16[512,2,96]{0,2,1:T(8,128)(2,1)}, u32[]{:S(2)}) copy-start(bf16[512,2,96]{0,2,1:T(8,128)(2,1)} %slice.124) | copy-start | bytes 589828
  65.8 2.5 %copy-start.11 = (pred[256,512]{1,0:T(8,128)(4,1)S(1)}, pred[256,512]{1,0:T(8,128)(4,1)}, u32[]{:S(2)}) copy-start(pred[256,512]{1,0:T(8,128)(4,1)} %broadcast_compare_fusion.2) | copy-start | bytes 393220
  65.8 2.5 %copy-start.14 = (bf16[256,2,96]{0,2,1:T(8,128)(2,1)S(1)}, bf16[256,2,96]{0,2,1:T(8,128)(2,1)}, u32[]{:S(2)}) copy-start(bf16[256,2,96]{0,2,1:T(8,128)(2,1)} %slice.122) | copy-start | bytes 294916
  67.1 2.0 copy-start.12
  67.2 2.4 %copy-start.7 = (pred[256,768]{1,0:T(8,128)(4,1)S(1)}, pred[256,768]{1,0:T(8,128)(4,1)}, u32[]{:S(2)}) copy-start(pred[256,768]{1,0:T(8,128)(4,1)} %broadcast_compare_fusion.1) | copy-start | bytes 589828
  67.2 2.4 %copy-start.13 = (bf16[256,2,96]{0,2,1:T(8,128)(2,1)S(1)}, bf16[256,2,96]{0,2,1:T(8,128)(2,1)}, u32[]{:S(2)}) copy-start(bf16[256,2,96]{0,2,1:T(8,128)(2,1)} %slice.128) | copy-start | bytes 294916
  69.6 1.0 copy-start.6
  71.2 1.4 copy-start.16
  74.7 13.8 %all-to-all-start.3 = ((bf16[8,2,8192]{2,1,0:T(2,128)(2,1)}), bf16[8,2,8192]{2,1,0:T(2,128)(2,1)S(1)}, u32[]{:S(2)}, u32[]{:S(2)}) async-start(bf16[8,2,8192]{2,1,0:T(2,128)(2,1)} %reshape.673), calls=%async_computation.3 | async-start | bytes 524288 | tf_op jit(solution)/shard_map/all_to_all | solution.py:137
  88.9 0.8 copy-start.19
  89.3 1.0 copy-start.10
  90.4 4.0 %copy-start.17 = (f32[2048]{0:T(1024)S(1)}, f32[2048]{0:T(1024)}, u32[]{:S(2)}) copy-start(f32[2048]{0:T(1024)} %param.29) | copy-start | bytes 24580
  93.4 1.0 copy-start.1
  98.0 53.4 %copy-start.26 = (bf16[1,2048,512]{2,1,0:T(8,128)(2,1)S(1)}, bf16[1,2048,512]{2,1,0:T(8,128)(2,1)}, u32[]{:S(2)}) copy-start(bf16[1,2048,512]{2,1,0:T(8,128)(2,1)} %param.33) | copy-start | bytes 6291460
  150.1 1.3 copy-start.4
  159.9 3.8 %copy-start.23 = (f32[1,128,2]{1,2,0:T(2,128)S(1)}, f32[1,128,2]{1,2,0:T(2,128)}, u32[]{:S(2)}) copy-start(f32[1,128,2]{1,2,0:T(2,128)} %param.32) | copy-start | bytes 3076
  159.9 3.8 %copy-start.25 = (f32[1,128]{1,0:T(1,128)S(1)}, f32[1,128]{1,0:T(1,128)}, u32[]{:S(2)}) copy-start(f32[1,128]{1,0:T(1,128)} %param.31) | copy-start | bytes 1540
  159.9 52.5 %all-to-all-start.5 = ((bf16[32,16,2048]{2,1,0:T(8,128)(2,1)}), bf16[32,16,2048]{2,1,0:T(8,128)(2,1)}, u32[]{:S(2)}, u32[]{:S(2)}) async-start(bf16[32,16,2048]{2,1,0:T(8,128)(2,1)} %bitcast.194), calls=%async_computation.5 | async-start | bytes 4194304 | tf_op jit(solution)/shard_map/all_to_all | solution.py:165
  219.4 1.5 copy-start.2
where the time goes:
time: 224 us; the launch traced here: 223 us
  waiting for transfers between devices  63.7 us (28%)
  blocking collectives  52.1 us (23%)
  local copies, waits for them, and re-layouts  43.2 us (19%)
  starting transfers between devices  26.3 us (12%)
  matrix products  20.1 us (9%)
  other arithmetic  16.7 us (7%)
    all_to_all x1, blocking collectives, per_device(): lax.all_to_all(outgoing, ('sp', 'dp'), split_axis=0, concat_axis=0, tiled...  52.1 us
    all_to_all x1, waiting for transfers between devices, per_device(): lax.all_to_all(jnp.dot(hidden, down_weight[0], preferred_element_type=jnp...  48.6 us
    all_to_all x1, waiting for transfers between devices, per_device(): lax.all_to_all(keys_tok, 'sp', split_axis=1, concat_axis=0, tiled=True)  7.94 us
    unnamed x59, local copies, waits for them, and re-layouts  7.81 us
    all_to_all x1, starting transfers between devices, per_device(): lax.all_to_all(values_tok, 'sp', split_axis=1, concat_axis=0, tiled=True)  7.31 us
    all_to_all x1, waiting for transfers between devices, per_device(): lax.all_to_all(head_out, 'sp', split_axis=0, concat_axis=1, tiled=True)  6.67 us
    dot_general x1, matrix products, per_device(): jnp.dot(hidden, down_weight[0], preferred_element_type=jnp.float32)  6.28 us
    all_to_all x1, starting transfers between devices, per_device(): lax.all_to_all(keys_tok, 'sp', split_axis=1, concat_axis=0, tiled=True)  6.01 us
  transfers between devices with their start and end apart: 5, of which 4 were waited for; matrix products, arithmetic and copies ran while one was open for 14% of the time, Pallas kernels for 0%

commit v1 on v0

--- a/solution.py
+++ b/solution.py
@@ -1,6 +1,10 @@
+import functools
+
 import jax
 import jax.numpy as jnp
 from jax import lax
+from jax.experimental import pallas as pl
+from jax.experimental.pallas import tpu as pltpu
 from jax.sharding import PartitionSpec as P
 
 GROUPS = 4
@@ -77,6 +81,269 @@
     return jnp.concatenate(pieces, axis=0)
 
 
+def dot32(a, b):
+    return jnp.dot(a, b, preferred_element_type=jnp.float32)
+
+
+def dot_t(a, b):
+    return lax.dot_general(a, b, (((0,), (0,)), ((), ())), preferred_element_type=jnp.float32)
+
+
+def expert_kernel(
+    n_y,
+    n_dp,
+    cap,
+    rows,
+    normed_ref,
+    info_ref,
+    pick_ref,
+    stream_ref,
+    gate_hbm,
+    up_hbm,
+    down_hbm,
+    out_ref,
+    gate_ref,
+    up_ref,
+    down_ref,
+    out1,
+    in1,
+    out2,
+    arrive,
+    served,
+    back2,
+    merged,
+    home,
+    acc,
+    w_sem,
+    s1,
+    r1,
+    s2,
+    r2,
+    s3,
+    r3,
+    s4,
+    r4,
+    l_sem,
+):
+    peers = n_y * n_dp
+    width = normed_ref.shape[1]
+    sp = lax.axis_index("sp")
+    dp = lax.axis_index("dp")
+    plane = sp // n_y
+    row = sp % n_y
+    mine = row * n_dp + dp
+
+    def column(k):
+        return {"sp": ((plane + k) % GROUPS) * n_y + row, "dp": dp}
+
+    def peer(j):
+        other = (mine + j) % peers
+        return {"sp": plane * n_y + other // n_dp, "dp": other % n_dp}
+
+    loads = [
+        pltpu.make_async_copy(gate_hbm, gate_ref, w_sem.at[0]),
+        pltpu.make_async_copy(up_hbm, up_ref, w_sem.at[1]),
+        pltpu.make_async_copy(down_hbm, down_ref, w_sem.at[2]),
+    ]
+    for load in loads:
+        load.start()
+    barrier = pltpu.get_barrier_semaphore()
+    for k in range(1, GROUPS):
+        pl.semaphore_signal(barrier, inc=1, device_id=column(k), device_id_type=pl.DeviceIdType.MESH)
+    for j in range(1, peers):
+        pl.semaphore_signal(barrier, inc=1, device_id=peer(j), device_id_type=pl.DeviceIdType.MESH)
+
+    def remote(src, dst, send, recv, target):
+        return pltpu.make_async_remote_copy(
+            src_ref=src,
+            dst_ref=dst,
+            send_sem=send,
+            recv_sem=recv,
+            device_id=target,
+            device_id_type=pl.DeviceIdType.MESH,
+        )
+
+    first = {}
+
+    def pack(k, target):
+        picks = pick_ref[(plane + k) % GROUPS]
+        target[k, :, :width] = dot32(picks, normed_ref[...]).astype(jnp.bfloat16)
+        target[k, :, width:] = dot32(picks, info_ref[...]).astype(jnp.bfloat16)
+
+    for k in (2, 1, 3):
+        pack(k, out1)
+        if k == 2:
+            pl.semaphore_wait(barrier, GROUPS - 1 + peers - 1)
+        first[k] = remote(out1.at[k], in1.at[k], s1.at[k], r1.at[k], column(k))
+        first[k].start()
+    pack(0, in1)
+
+    def slots(k):
+        info = in1[k, :, width:].astype(jnp.float32)
+        place = lax.broadcasted_iota(jnp.int32, (rows, peers * cap), 1).astype(jnp.float32)
+        return place == info[:, 0:1], place == info[:, 1:2], info
+
+    second = {}
+
+    def scatter(k):
+        if k:
+            first[k].wait_recv()
+        at0, at1, _ = slots(k)
+        choose = (at0.astype(jnp.float32) + at1.astype(jnp.float32)).astype(jnp.bfloat16)
+        placed = dot_t(choose, in1[k, :, :width]).astype(jnp.bfloat16)
+        for e in range(peers):
+            out2[k, e] = placed[e * cap : (e + 1) * cap]
+        second[k] = [
+            remote(
+                out2.at[k, (mine + j) % peers], arrive.at[k, j], s2.at[k, j], r2.at[k, j], peer(j)
+            )
+            for j in range(1, peers)
+        ]
+        for copy in second[k]:
+            copy.start()
+        arrive[k, 0] = out2[k, mine]
+
+    third = {}
+
+    def serve(k):
+        for copy in second[k]:
+            copy.wait_recv()
+        if k == 0:
+            for load in loads:
+                load.wait()
+        given = arrive[k].reshape(peers * cap, width)
+        gate_act = dot32(given, gate_ref[...])
+        upward = dot32(given, up_ref[...])
+        hidden = (gate_act * (1.0 / (1.0 + jnp.exp(-gate_act))) * upward).astype(jnp.bfloat16)
+        result = dot32(hidden, down_ref[...]).astype(jnp.bfloat16)
+        for j in range(peers):
+            served[k, j] = result[j * cap : (j + 1) * cap]
+        third[k] = [
+            remote(
+                served.at[k, j], back2.at[k, mine], s3.at[k, j], r3.at[k, peers - j], peer(peers - j)
+            )
+            for j in range(1, peers)
+        ]
+        for copy in third[k]:
+            copy.start()
+        back2[k, mine] = served[k, 0]
+
+    fourth = {}
+
+    def merge(k):
+        for copy in third[k]:
+            copy.wait_recv()
+        at0, at1, info = slots(k)
+        high = jnp.where(at0, info[:, 2:3], 0.0) + jnp.where(at1, info[:, 4:5], 0.0)
+        low = jnp.where(at0, info[:, 3:4], 0.0) + jnp.where(at1, info[:, 5:6], 0.0)
+        got = back2[k].reshape(peers * cap, width)
+        total = dot32(high.astype(jnp.bfloat16), got) + dot32(low.astype(jnp.bfloat16), got)
+        if k:
+            merged[k] = total.astype(jnp.bfloat16)
+            fourth[k] = remote(merged.at[k], home.at[k], s4.at[k], r4.at[k], column(GROUPS - k))
+            fourth[k].start()
+        else:
+            acc[...] = stream_ref[...] + dot_t(pick_ref[plane], total.astype(jnp.bfloat16))
+
+    scatter(0)
+    scatter(1)
+    serve(0)
+    scatter(3)
+    merge(0)
+    serve(1)
+    scatter(2)
+    merge(1)
+    serve(3)
+    serve(2)
+    merge(3)
+    merge(2)
+    for k in (1, 3, 2):
+        fourth[k].wait_recv()
+        acc[...] += dot_t(pick_ref[(plane + k) % GROUPS], home[k])
+    out_ref[...] = acc[...].astype(jnp.bfloat16)
+    for k in range(GROUPS):
+        if k:
+            first[k].wait_send()
+            fourth[k].wait_send()
+        for copy in second[k] + third[k]:
+            copy.wait_send()
+
+
+def routed(normed, stream, choice, group_prob, share, gate, up, down, expert_total):
+    tok_rows, width = normed.shape
+    n_y = lax.axis_size("sp") // GROUPS
+    n_dp = lax.axis_size("dp")
+    per_group = expert_total // GROUPS
+    cap = tok_rows * GROUPS // expert_total
+    rows = per_group * cap // choice.shape[1]
+    group = choice[:, 0] // per_group
+    order = jnp.arange(tok_rows, dtype=jnp.int32)
+    before = order[None, :] < order[:, None]
+    rank = jnp.sum((before & (group[None, :] == group[:, None])).astype(jnp.int32), axis=1)
+    line = group * rows + rank
+    pick = (
+        (line[None, :] == jnp.arange(GROUPS * rows, dtype=jnp.int32)[:, None])
+        .astype(jnp.bfloat16)
+        .reshape(GROUPS, rows, tok_rows)
+    )
+    route = group_prob[:, None] * share / jnp.sum(share, axis=-1, keepdims=True)
+    earlier = jnp.sum(
+        (
+            before[:, None, :, None] & (choice[:, :, None, None] == choice[None, None, :, :])
+        ).astype(jnp.int32),
+        axis=(2, 3),
+    )
+    position = (choice - group[:, None] * per_group) * cap + earlier
+    high = lax.reduce_precision(route, 8, 7)
+    low = route - high
+    columns = jnp.concatenate(
+        [
+            position.astype(jnp.float32),
+            jnp.stack([high[:, 0], low[:, 0], high[:, 1], low[:, 1]], axis=1),
+            jnp.zeros((tok_rows, 122), jnp.float32),
+        ],
+        axis=1,
+    ).astype(jnp.bfloat16)
+    hidden = gate.shape[1]
+    bf = jnp.bfloat16
+    vmem = pl.BlockSpec(memory_space=pltpu.VMEM)
+    hbm = pl.BlockSpec(memory_space=pl.ANY)
+    dma = pltpu.SemaphoreType.DMA
+    return pl.pallas_call(
+        functools.partial(expert_kernel, n_y, n_dp, cap, rows),
+        out_shape=jax.ShapeDtypeStruct((tok_rows, width), bf),
+        in_specs=[vmem] * 4 + [hbm] * 3,
+        out_specs=vmem,
+        scratch_shapes=[
+            pltpu.VMEM((width, hidden), bf),
+            pltpu.VMEM((width, hidden), bf),
+            pltpu.VMEM((hidden, width), bf),
+            pltpu.VMEM((GROUPS, rows, width + 128), bf),
+            pltpu.VMEM((GROUPS, rows, width + 128), bf),
+            pltpu.VMEM((GROUPS, per_group, cap, width), bf),
+            pltpu.VMEM((GROUPS, per_group, cap, width), bf),
+            pltpu.VMEM((GROUPS, per_group, cap, width), bf),
+            pltpu.VMEM((GROUPS, per_group, cap, width), bf),
+            pltpu.VMEM((GROUPS, rows, width), bf),
+            pltpu.VMEM((GROUPS, rows, width), bf),
+            pltpu.VMEM((tok_rows, width), jnp.float32),
+            dma((3,)),
+            dma((GROUPS,)),
+            dma((GROUPS,)),
+            dma((GROUPS, per_group)),
+            dma((GROUPS, per_group)),
+            dma((GROUPS, per_group)),
+            dma((GROUPS, per_group)),
+            dma((GROUPS,)),
+            dma((GROUPS,)),
+            dma((1,)),
+        ],
+        compiler_params=pltpu.CompilerParams(
+            collective_id=0, has_side_effects=True, vmem_limit_bytes=60 * 1024 * 1024
+        ),
+    )(normed, columns, pick, stream, gate, up, down)
+
+
 def per_device(
     residual,
     query,
@@ -143,45 +410,17 @@
     )
     normed = rms_scale(stream, ffn_gain).astype(jnp.bfloat16)
     expert_total = seq_devices * lax.axis_size("dp")
-    capacity = tok_rows * GROUPS // expert_total
-    picked = expert_choice[0].reshape(-1)
-    one_hot = (picked[:, None] == jnp.arange(expert_total, dtype=jnp.int32)[None, :]).astype(
-        jnp.int32
-    )
-    earlier = jnp.cumsum(one_hot, axis=0) - one_hot
-    slot_rank = jnp.sum(earlier * one_hot, axis=1)
-    target = picked * capacity + slot_rank
-    source_row = jnp.arange(picked.shape[0], dtype=jnp.int32) // expert_choice.shape[2]
-    slot_token = (
-        jnp.full((expert_total * capacity,), tok_rows, jnp.int32).at[target].set(source_row)
-    )
-    padded = jnp.concatenate([normed, jnp.zeros((1, model_width), jnp.bfloat16)], axis=0)
-    outgoing = padded[slot_token].reshape(expert_total, capacity, model_width)
-    arrived = lax.all_to_all(outgoing, ("sp", "dp"), split_axis=0, concat_axis=0, tiled=True)
-    flat_rows = arrived.reshape(-1, model_width)
-    gate_act = jnp.dot(flat_rows, gate_weight[0], preferred_element_type=jnp.float32)
-    upward = jnp.dot(flat_rows, up_weight[0], preferred_element_type=jnp.float32)
-    hidden = (jax.nn.silu(gate_act) * upward).astype(jnp.bfloat16)
-    returned = lax.all_to_all(
-        jnp.dot(hidden, down_weight[0], preferred_element_type=jnp.float32)
-        .astype(jnp.bfloat16)
-        .reshape(arrived.shape),
-        ("sp", "dp"),
-        split_axis=0,
-        concat_axis=0,
-        tiled=True,
-    )
-    gathered_rows = returned.reshape(-1, model_width)[target].reshape(
-        tok_rows, expert_choice.shape[2], model_width
-    )
-    expert_share = expert_prob[0]
-    route_weight = (
-        group_prob[0][:, None] * expert_share / jnp.sum(expert_share, axis=-1, keepdims=True)
-    )
-    routed_sum = route_weight[:, 0:1] * gathered_rows[:, 0].astype(jnp.float32) + route_weight[
-        :, 1:2
-    ] * gathered_rows[:, 1].astype(jnp.float32)
-    return (stream + routed_sum).astype(jnp.bfloat16)[None]
+    return routed(
+        normed,
+        stream,
+        expert_choice[0],
+        group_prob[0],
+        expert_prob[0],
+        gate_weight[0],
+        up_weight[0],
+        down_weight[0],
+        expert_total,
+    )[None]
 
 
 def solution(mesh):

time: 224 us -> 159 us (0.71)
  Pallas kernels: 0 us -> 80.6 us
  blocking collectives: 52.1 us -> 0 us
  waiting for transfers between devices: 63.7 us -> 30.3 us
  local copies, waits for them, and re-layouts: 43.2 us -> 12.1 us
  matrix products: 20.1 us -> 8.33 us
  other arithmetic: 16.7 us -> 8.39 us
  starting transfers between devices: 26.3 us -> 18.3 us
    pallas_call x0 -> x1, Pallas kernels: none -> 80.6 us  [routed(): pl.pallas_call(functools.partial(expert_kernel, n_y, n_dp, cap, rows), ou...]
    all_to_all x1 -> x0, blocking collectives: 52.1 us -> none  [per_device(): lax.all_to_all(outgoing, ('sp', 'dp'), split_axis=0, concat_axis=0, tiled...]
    all_to_all x1 -> x0, waiting for transfers between devices: 48.6 us -> none  [per_device(): lax.all_to_all(jnp.dot(hidden, down_weight[0], preferred_element_type=jnp...]
    gather x2 -> x0, local copies, waits for them, and re-layouts: 8.56 us -> none  [the longest x1 5.21 us: per_device(): returned.reshape(-1, model_width)[target]]
    dot_general x2 -> x0, matrix products: 8.54 us -> none  [the longest x1 6.28 us: per_device(): jnp.dot(hidden, down_weight[0], preferred_element_type=jnp.float32)]
    all_to_all x1, waiting for transfers between devices: 0.44 us -> 8.87 us  [per_device(): lax.all_to_all(queries_tok, 'sp', split_axis=1, concat_axis=0, tiled=True)]
    slice x5, local copies, waits for them, and re-layouts: 5.04 us -> 0.61 us  [attend(): keys_head[:last_row]]
    all_to_all x1, waiting for transfers between devices: 0.01 us -> 4.05 us  [per_device(): lax.all_to_all(values_tok, 'sp', split_axis=1, concat_axis=0, tiled=True)]
  transfers between devices with their start and end apart: 5 -> 4, of which waited for: 4 -> 4; matrix products, arithmetic and copies ran while one was open for 14% -> 6% of each run, Pallas kernels for 0% -> 0%
where the time goes in v1:
time: 159 us
  Pallas kernels  80.6 us (51%)
  waiting for transfers between devices  30.3 us (19%)
  starting transfers between devices  18.3 us (12%)
  local copies, waits for them, and re-layouts  12.1 us (8%)
  other arithmetic  8.39 us (5%)
  matrix products  8.33 us (5%)
    pallas_call x1, Pallas kernels, routed(): pl.pallas_call(functools.partial(expert_kernel, n_y, n_dp, cap, rows), ou...  80.6 us
    all_to_all x1, waiting for transfers between devices, per_device(): lax.all_to_all(keys_tok, 'sp', split_axis=1, concat_axis=0, tiled=True)  10.3 us
    all_to_all x1, waiting for transfers between devices, per_device(): lax.all_to_all(queries_tok, 'sp', split_axis=1, concat_axis=0, tiled=True)  8.87 us
    all_to_all x1, starting transfers between devices, per_device(): lax.all_to_all(values_tok, 'sp', split_axis=1, concat_axis=0, tiled=True)  7.45 us
    all_to_all x1, waiting for transfers between devices, per_device(): lax.all_to_all(head_out, 'sp', split_axis=0, concat_axis=1, tiled=True)  7.08 us
    unnamed x39, local copies, waits for them, and re-layouts  5.09 us
    all_to_all x1, waiting for transfers between devices, per_device(): lax.all_to_all(values_tok, 'sp', split_axis=1, concat_axis=0, tiled=True)  4.05 us
    all_to_all x1, starting transfers between devices, per_device(): lax.all_to_all(queries_tok, 'sp', split_axis=1, concat_axis=0, tiled=True)  3.64 us
  transfers between devices with their start and end apart: 4, of which 4 were waited for; matrix products, arithmetic and copies ran while one was open for 6% of the time, Pallas kernels for 0%

profile of v1, /device:TPU:0, one launch (start us, length us, event | category | flops | bytes accessed | tf_op | source)
XLA Modules:
  0.0 158.7 jit_solution(17716255233454481770)
XLA Ops:
  0.0 1.0 fusion.34
  1.1 1.1 convolution_convert_fusion.1
  2.2 0.8 copy.74
  3.0 7.4 %all-to-all-start = ((bf16[128,16,64]{0,2,1:T(8,128)(2,1)}), bf16[128,16,64]{0,2,1:T(8,128)(2,1)S(1)}, u32[]{:S(2)}, u32[]{:S(2)}) async-start(bf16[128,16,64]{0,2,1:T(8,128)(2,1)} %bitcast.3), calls=%async_computation | async-start | bytes 524288 | tf_op jit(solution)/shard_map/all_to_all | solution.py:401
  10.5 0.8 copy.84
  11.3 0.2 fusion.54
  11.7 0.3 fusion.7
  11.9 0.2 copy.78
  12.3 0.2 copy.76
  12.5 0.1 fusion.22
  12.7 0.3 fusion.23
  13.1 0.1 multiply_cosine_fusion
  13.2 0.2 convert_reduce_fusion
  13.4 0.2 convert_reduce_fusion.1
  13.7 0.8 pad_maximum_fusion.2
  14.6 0.8 pad_maximum_fusion.1
  15.4 4.1 %all-to-all-done = bf16[128,16,64]{0,2,1:T(8,128)(2,1)S(1)} async-done(((bf16[128,16,64]{0,2,1:T(8,128)(2,1)}), bf16[128,16,64]{0,2,1:T(8,128)(2,1)S(1)}, u32[]{:S(2)}, u32[]{:S(2)}) %all-to-all-start) | async-done | bytes 262176 | tf_op jit(solution)/shard_map/all_to_all | solution.py:401
  19.4 3.6 %all-to-all-start.2 = ((bf16[128,16,96]{0,2,1:T(8,128)(2,1)}), bf16[128,16,96]{0,2,1:T(8,128)(2,1)S(1)}, u32[]{:S(2)}, u32[]{:S(2)}) async-start(bf16[128,16,96]{0,2,1:T(8,128)(2,1)} %pad_maximum_fusion.2), calls=%async_computation.2 | async-start | bytes 786432 | tf_op jit(solution)/shard_map/all_to_all | solution.py:400
  23.0 0.1 copy.89
  23.2 0.1 broadcast_compare_fusion.3
  23.3 0.1 fusion.37
  23.4 0.7 fusion.56
  24.1 10.3 %all-to-all-done.2 = bf16[128,16,96]{0,2,1:T(8,128)(2,1)S(1)} async-done(((bf16[128,16,96]{0,2,1:T(8,128)(2,1)}), bf16[128,16,96]{0,2,1:T(8,128)(2,1)S(1)}, u32[]{:S(2)}, u32[]{:S(2)}) %all-to-all-start.2) | async-done | bytes 393248 | tf_op jit(solution)/shard_map/all_to_all | solution.py:400
  34.4 3.6 %all-to-all-start.1 = ((bf16[128,16,96]{0,2,1:T(8,128)(2,1)}), bf16[128,16,96]{0,2,1:T(8,128)(2,1)S(1)}, u32[]{:S(2)}, u32[]{:S(2)}) async-start(bf16[128,16,96]{0,2,1:T(8,128)(2,1)} %pad_maximum_fusion.1), calls=%async_computation.1 | async-start | bytes 786432 | tf_op jit(solution)/shard_map/all_to_all | solution.py:399
  38.0 0.1 broadcast_compare_fusion.2
  38.2 0.2 broadcast_compare_fusion.1
  38.3 0.2 broadcast_compare_fusion
  38.6 0.2 copy.98
  38.8 0.8 all_to_all.53
  39.8 0.2 slice.127
  40.0 0.3 copy.96
  40.4 0.2 all_to_all.54
  40.7 8.9 %all-to-all-done.1 = bf16[128,16,96]{0,2,1:T(8,128)(2,1)S(1)} async-done(((bf16[128,16,96]{0,2,1:T(8,128)(2,1)}), bf16[128,16,96]{0,2,1:T(8,128)(2,1)S(1)}, u32[]{:S(2)}, u32[]{:S(2)}) %all-to-all-start.1) | async-done | bytes 393248 | tf_op jit(solution)/shard_map/all_to_all | solution.py:399
  49.5 0.3 copy.97
  49.8 0.3 fusion.55
  50.3 0.4 slice.131
  50.8 0.3 fusion.60
  51.2 0.2 fusion.13
  51.4 0.5 fusion.59
  51.9 0.3 fusion.20
  52.2 0.4 fusion.14
  52.7 0.6 fusion.58
  53.2 0.4 fusion.3
  53.7 0.6 fusion.15
  54.2 0.7 fusion
  54.9 0.7 fusion.1
  55.6 0.7 fusion.12
  56.3 0.4 copy.81
  56.7 1.1 reshape.647
  57.8 3.6 %all-to-all-start.3 = ((bf16[8,2,8192]{2,1,0:T(2,128)(2,1)}), bf16[8,2,8192]{2,1,0:T(2,128)(2,1)S(1)}, u32[]{:S(2)}, u32[]{:S(2)}) async-start(bf16[8,2,8192]{2,1,0:T(2,128)(2,1)} %reshape.647), calls=%async_computation.3 | async-start | bytes 524288 | tf_op jit(solution)/shard_map/all_to_all | solution.py:404
  61.5 0.1 copy.90
  61.6 0.7 concatenate.23.info_ref
  62.4 0.7 compare_convert_fusion.pick_ref
  63.1 7.1 %all-to-all-done.3 = bf16[8,2,8192]{2,1,0:T(2,128)(2,1)S(1)} async-done(((bf16[8,2,8192]{2,1,0:T(2,128)(2,1)}), bf16[8,2,8192]{2,1,0:T(2,128)(2,1)S(1)}, u32[]{:S(2)}, u32[]{:S(2)}) %all-to-all-start.3) | async-done | bytes 262176 | tf_op jit(solution)/shard_map/all_to_all | solution.py:404
  70.2 0.3 reshape.648
  70.5 0.4 copy.82
  71.1 0.1 copy.92
  71.2 0.1 copy.83
  71.3 0.2 fusion.28
  71.5 0.5 copy-done.3
  72.0 3.0 %multiply_reduce_fusion = (f32[128]{0:T(128)S(1)}, f32[128,2048]{1,0:T(8,128)S(1)}) fusion(bf16[128,1024]{0,1:T(8,128)(2,1)S(1)} %fusion.28, bf16[1024,2048]{1,0:T(8,128)(2,1)} %param.28, bf16[1,128,2048]{2,1,0:T(8,128)(2,1)S(1)} %copy-done.3), kind=kOutput, calls=%fused_computation.30 | convolution fusion | flops 537919360 | bytes 6029824 | tf_op jit(solution)/shard_map/dot_general | solution.py:408
  75.0 1.1 multiply_convert_fusion.normed_ref
  76.2 80.6 %shard_map.172 = bf16[128,2048]{1,0:T(8,128)(2,1)} custom-call(bf16[128,2048]{1,0:T(8,128)(2,1)} %multiply_convert_fusion.normed_ref, bf16[128,128]{1,0:T(8,128)(2,1)} %concatenate.23.info_ref, bf16[4,64,128]{2,1,0:T(8,128)(2,1)} %compare_convert_fusion.pick_ref, f32[128,2048]{1,0:T(8,128)} %copy-done.1, bf16[2048,512]{1,0:T(8,128)(2,1)} %bitcast.148, ...), custom_call_target="tpu_custom_call" | custom-call | tf_op jit(solution)/shard_map/pallas_call | solution.py:312
  156.8 1.9 %copy.100 = bf16[1,128,2048]{2,1,0:T(8,128)(2,1)} copy(bf16[1,128,2048]{2,1,0:T(8,128)(2,1)} %bitcast.145) | data formatting | bytes 1048576
  (78 shorter events, 1.7 us)
Async XLA Ops:
  0.0 1.1 copy-start
  0.0 11.6 %copy-start.2 = (bf16[1,128,256]{2,1,0:T(8,128)(2,1)S(1)}, bf16[1,128,256]{2,1,0:T(8,128)(2,1)}, u32[]{:S(2)}) copy-start(bf16[1,128,256]{2,1,0:T(8,128)(2,1)} %param.20) | copy-start | bytes 196612
  0.0 11.6 %copy-start.11 = (f32[256]{0:T(256)S(1)}, f32[256]{0:T(256)}, u32[]{:S(2)}) copy-start(f32[256]{0:T(256)} %param.22) | copy-start | bytes 3076
  0.0 11.6 %copy-start.4 = (bf16[256,1024]{1,0:T(8,128)(2,1)S(1)}, bf16[256,1024]{1,0:T(8,128)(2,1)}, u32[]{:S(2)}) copy-start(bf16[256,1024]{1,0:T(8,128)(2,1)} %param.25) | copy-start | bytes 1572868
  1.1 11.1 %copy-start.9 = (bf16[1,128,32]{1,2,0:T(8,128)(2,1)S(1)}, bf16[1,128,32]{1,2,0:T(8,128)(2,1)}, u32[]{:S(2)}) copy-start(bf16[1,128,32]{1,2,0:T(8,128)(2,1)} %param.21) | copy-start | bytes 24580
  3.0 9.2 %copy-start.5 = (bf16[1,128,1536]{2,1,0:T(8,128)(2,1)S(1)}, bf16[1,128,1536]{2,1,0:T(8,128)(2,1)}, u32[]{:S(2)}) copy-start(bf16[1,128,1536]{2,1,0:T(8,128)(2,1)} %param.19) | copy-start | bytes 1179652
  3.0 16.4 %all-to-all-start = ((bf16[128,16,64]{0,2,1:T(8,128)(2,1)}), bf16[128,16,64]{0,2,1:T(8,128)(2,1)S(1)}, u32[]{:S(2)}, u32[]{:S(2)}) async-start(bf16[128,16,64]{0,2,1:T(8,128)(2,1)} %bitcast.3), calls=%async_computation | async-start | bytes 524288 | tf_op jit(solution)/shard_map/all_to_all | solution.py:401
  11.6 1.0 copy-start.13
  11.6 1.0 copy-start.14
  13.0 10.0 %copy-start.12 = (f32[1,128,2]{1,2,0:T(2,128)S(1)}, f32[1,128,2]{1,2,0:T(2,128)}, u32[]{:S(2)}) copy-start(f32[1,128,2]{1,2,0:T(2,128)} %param.32) | copy-start | bytes 3076
  13.0 10.3 %copy-start.15 = (f32[1,128]{1,0:T(1,128)S(1)}, f32[1,128]{1,0:T(1,128)}, u32[]{:S(2)}) copy-start(f32[1,128]{1,0:T(1,128)} %param.31) | copy-start | bytes 1540
  19.4 15.0 %all-to-all-start.2 = ((bf16[128,16,96]{0,2,1:T(8,128)(2,1)}), bf16[128,16,96]{0,2,1:T(8,128)(2,1)S(1)}, u32[]{:S(2)}, u32[]{:S(2)}) async-start(bf16[128,16,96]{0,2,1:T(8,128)(2,1)} %pad_maximum_fusion.2), calls=%async_computation.2 | async-start | bytes 786432 | tf_op jit(solution)/shard_map/all_to_all | solution.py:400
  34.4 15.1 %all-to-all-start.1 = ((bf16[128,16,96]{0,2,1:T(8,128)(2,1)}), bf16[128,16,96]{0,2,1:T(8,128)(2,1)S(1)}, u32[]{:S(2)}, u32[]{:S(2)}) async-start(bf16[128,16,96]{0,2,1:T(8,128)(2,1)} %pad_maximum_fusion.1), calls=%async_computation.1 | async-start | bytes 786432 | tf_op jit(solution)/shard_map/all_to_all | solution.py:399
  54.2 1.4 copy-start.6
  56.3 5.3 %copy-start.7 = (bf16[128,1]{1,0:T(8,128)(2,1)S(1)}, bf16[128,1]{1,0:T(8,128)(2,1)}, u32[]{:S(2)}) copy-start(bf16[128,1]{1,0:T(8,128)(2,1)} %get-tuple-element.39) | copy-start | bytes 772
  57.8 12.3 %all-to-all-start.3 = ((bf16[8,2,8192]{2,1,0:T(2,128)(2,1)}), bf16[8,2,8192]{2,1,0:T(2,128)(2,1)S(1)}, u32[]{:S(2)}, u32[]{:S(2)}) async-start(bf16[8,2,8192]{2,1,0:T(2,128)(2,1)} %reshape.647), calls=%async_computation.3 | async-start | bytes 524288 | tf_op jit(solution)/shard_map/all_to_all | solution.py:404
  70.5 0.8 copy-start.10
  70.9 1.0 copy-start.3
  72.0 3.0 %copy-start.8 = (f32[2048]{0:T(1024)S(1)}, f32[2048]{0:T(1024)}, u32[]{:S(2)}) copy-start(f32[2048]{0:T(1024)} %param.29) | copy-start | bytes 24580
  75.0 1.2 copy-start.1

commit v2 on v1

--- a/solution.py
+++ b/solution.py
@@ -14,71 +14,10 @@
 eps = 1e-06
 
 
-def rms_scale(vector, gains):
-    return vector * lax.rsqrt(jnp.mean(vector * vector, axis=-1, keepdims=True) + eps) * gains
-
-
-def rotate(vector, phases):
-    half_width = vector.shape[-1] // 2
-    lower_half = vector[..., :half_width]
-    upper_half = vector[..., half_width:]
-    cos_table = jnp.cos(phases)
-    sin_table = jnp.sin(phases)
-    return jnp.concatenate(
-        [
-            lower_half * cos_table - upper_half * sin_table,
-            upper_half * cos_table + lower_half * sin_table,
-        ],
-        axis=-1,
-    )
-
-
 def angles(offset, span_count, rope_width):
     position = (offset + jnp.arange(span_count, dtype=jnp.int32)).astype(jnp.float32)
     frequency = 10000.0 ** (-2.0 * jnp.arange(rope_width // 2, dtype=jnp.float32) / rope_width)
     return position[:, None] * frequency[None, :]
-
-
-def head_vectors(nope_part, rope_part, gains, phases):
-    normed_all = rms_scale(jnp.concatenate([nope_part, rope_part], axis=-1), gains)
-    split_at = nope_part.shape[-1]
-    turned = rotate(normed_all[..., split_at:], phases[:, None, :])
-    return jnp.concatenate([normed_all[..., :split_at], turned], axis=-1).astype(jnp.bfloat16)
-
-
-def attend(queries_head, keys_head, values_head):
-    length = queries_head.shape[0]
-    blocks_count = max(4, length // 1024)
-    block_rows = length // blocks_count
-    score_scale = queries_head.shape[-1] ** (-0.5)
-    pieces = []
-    for block_index in range(blocks_count):
-        first_row = block_index * block_rows
-        last_row = first_row + block_rows
-        scores = (
-            jnp.einsum(
-                "qhd,khd->hqk",
-                queries_head[first_row:last_row],
-                keys_head[:last_row],
-                preferred_element_type=jnp.float32,
-            )
-            * score_scale
-        )
-        query_pos = first_row + jnp.arange(block_rows, dtype=jnp.int32)
-        key_pos = jnp.arange(last_row, dtype=jnp.int32)
-        allowed = key_pos[None, :] // SPAN <= query_pos[:, None] // SPAN
-        scores = jnp.where(allowed[None], scores, -1e30)
-        row_top = jnp.max(scores, axis=-1, keepdims=True)
-        raised = jnp.exp(scores - row_top)
-        row_sum = jnp.sum(raised, axis=-1)
-        summed = jnp.einsum(
-            "hqk,khd->qhd",
-            raised.astype(jnp.bfloat16),
-            values_head[:last_row],
-            preferred_element_type=jnp.float32,
-        )
-        pieces.append((summed / row_sum.T[:, :, None]).astype(jnp.bfloat16))
-    return jnp.concatenate(pieces, axis=0)
 
 
 def dot32(a, b):
@@ -267,6 +206,339 @@
             fourth[k].wait_send()
         for copy in second[k] + third[k]:
             copy.wait_send()
+
+
+def attention_kernel(
+    n_sp,
+    n_y,
+    heads,
+    nope,
+    rope,
+    value_width,
+    query_ref,
+    packed_ref,
+    latent_gain_ref,
+    query_gain_ref,
+    query_swap_ref,
+    key_gain_ref,
+    key_swap_ref,
+    cos_ref,
+    sin_ref,
+    key_weight_ref,
+    value_weight_ref,
+    residual_ref,
+    mix_gain_ref,
+    ffn_gain_ref,
+    out_weight_hbm,
+    stream_ref,
+    normed_ref,
+    out_weight_ref,
+    queries_in,
+    packed_in,
+    queries,
+    keys,
+    values,
+    heads_out,
+    token_in,
+    mixed,
+    w_sem,
+    sq,
+    rq,
+    sz,
+    rz,
+    sy,
+    ry,
+    so,
+    ro,
+):
+    bf = jnp.bfloat16
+    tok = residual_ref.shape[0]
+    length = n_sp * tok
+    qk = nope + rope
+    lat = packed_ref.shape[1]
+    me = lax.axis_index("sp")
+    plane = me // n_y
+    row = me % n_y
+    load = pltpu.make_async_copy(out_weight_hbm, out_weight_ref, w_sem.at[0])
+    load.start()
+
+    def remote(src, dst, send, recv, target):
+        return pltpu.make_async_remote_copy(
+            src_ref=src,
+            dst_ref=dst,
+            send_sem=send,
+            recv_sem=recv,
+            device_id={"sp": target},
+            device_id_type=pl.DeviceIdType.MESH,
+        )
+
+    barrier = pltpu.get_barrier_semaphore()
+    for j in range(1, n_sp):
+        pl.semaphore_signal(
+            barrier,
+            inc=1,
+            device_id={"sp": (me + j) % n_sp},
+            device_id_type=pl.DeviceIdType.MESH,
+        )
+    pl.semaphore_wait(barrier, n_sp - 1)
+
+    down = []
+    for k in range(1, GROUPS):
+        target = ((plane + k) % GROUPS) * n_y + row
+        down.append(remote(packed_ref, packed_in.at[me], sz.at[k], rz.at[k], target))
+        down[-1].start()
+    across = []
+
+    def spread(k, source):
+        index = ((plane + GROUPS - k) % GROUPS) * n_y + row
+        for m in range(1, n_y):
+            target = plane * n_y + (row + m) % n_y
+            across.append(remote(source, packed_in.at[index], sy.at[k, m], ry.at[k, m], target))
+            across[-1].start()
+
+    spread(0, packed_ref)
+    sent = []
+    for j in range(1, n_sp):
+        target = (me + j) % n_sp
+        sent.append(remote(query_ref.at[target], queries_in.at[me], sq.at[j], rq.at[j], target))
+        sent[-1].start()
+    packed_in[me] = packed_ref[...]
+    queries_in[me] = query_ref[me]
+    for k in range(1, GROUPS):
+        down[k - 1].wait_recv()
+        spread(k, packed_in.at[((plane + GROUPS - k) % GROUPS) * n_y + row])
+    for copy in across:
+        copy.wait_recv()
+
+    def selector(rows, columns, source):
+        i = lax.broadcasted_iota(jnp.int32, (rows, columns), 0)
+        c = lax.broadcasted_iota(jnp.int32, (rows, columns), 1)
+        return (i == source(c)).astype(jnp.float32).astype(bf)
+
+    half = rope // 2
+
+    def swapped(c):
+        return jnp.where(c < nope, -1, jnp.where(c < nope + half, c + half, c - half))
+
+    def shape_head(plain, turned, gain, swap_gain, rows):
+        scale = lax.rsqrt(jnp.sum(plain * plain, axis=-1, keepdims=True) / qk + eps)
+        return (
+            plain * scale * gain * cos_ref[rows, :] + turned * scale * swap_gain * sin_ref[rows, :]
+        ).astype(bf)
+
+    strips = lat // rope
+    strip_rows = tok // strips
+
+    def prepare(s, carry):
+        rows = pl.ds(pl.multiple_of(s * tok, tok), tok)
+        block = packed_in[s]
+        raw = block[:tok].astype(jnp.float32)
+        scale = lax.rsqrt(jnp.mean(raw * raw, axis=-1, keepdims=True) + eps)
+        latent = (raw * scale * latent_gain_ref[...]).astype(bf)
+        values[rows, :] = dot32(latent, value_weight_ref[...]).astype(bf)
+        part = dot32(latent, key_weight_ref[...]).astype(bf)
+        tail = block[tok:]
+        plain_rope = jnp.concatenate(
+            [
+                dot32(tail, selector(lat, qk, lambda c: jnp.where(c < nope, -1, c - nope + i * rope)))
+                for i in range(strips)
+            ],
+            axis=0,
+        )
+        turned = jnp.concatenate(
+            [
+                dot32(
+                    tail,
+                    selector(
+                        lat, qk, lambda c: jnp.where(c < nope, -1, swapped(c) - nope + i * rope)
+                    ),
+                )
+                for i in range(strips)
+            ],
+            axis=0,
+        )
+        for h in range(heads):
+            plain = plain_rope + dot32(
+                part, selector(heads * nope, qk, lambda c: jnp.where(c < nope, c + h * nope, -1))
+            )
+            keys[h, rows, :] = shape_head(
+                plain, turned, key_gain_ref[...], key_swap_ref[...], rows
+            )
+        return carry
+
+    lax.fori_loop(0, n_sp, prepare, 0)
+    for copy in sent:
+        copy.wait_recv()
+
+    def prepare_queries(s, carry):
+        rows = pl.ds(pl.multiple_of(s * tok, tok), tok)
+        raw = queries_in[s]
+        for h in range(heads):
+            plain = dot32(raw, selector(heads * qk, qk, lambda c: c + h * qk))
+            turned = dot32(
+                raw,
+                selector(
+                    heads * qk, qk, lambda c: jnp.where(c < nope, -1, swapped(c) + h * qk)
+                ),
+            )
+            queries[h, rows, :] = shape_head(
+                plain, turned, query_gain_ref[...], query_swap_ref[...], rows
+            )
+        return carry
+
+    lax.fori_loop(0, n_sp, prepare_queries, 0)
+
+    blocks = 4
+    block_rows = length // blocks
+    for b in range(blocks):
+        first_row = b * block_rows
+        last_row = first_row + block_rows
+        total = None
+        lane = lax.broadcasted_iota(jnp.int32, (block_rows, heads * value_width), 1)
+        q_pos = first_row + lax.broadcasted_iota(jnp.int32, (block_rows, last_row), 0)
+        k_pos = lax.broadcasted_iota(jnp.int32, (block_rows, last_row), 1)
+        allowed = k_pos // SPAN <= q_pos // SPAN
+        for h in range(heads):
+            scores = lax.dot_general(
+                queries[h, first_row:last_row],
+                keys[h, :last_row],
+                (((1,), (1,)), ((), ())),
+                preferred_element_type=jnp.float32,
+            ) * (qk ** (-0.5))
+            scores = jnp.where(allowed, scores, -1e30)
+            raised = jnp.exp(scores - jnp.max(scores, axis=-1, keepdims=True))
+            row_sum = jnp.sum(raised, axis=-1, keepdims=True)
+            mine = dot32(raised.astype(bf), values[:last_row]) / row_sum
+            total = mine if total is None else jnp.where(lane < h * value_width, total, mine)
+        total = total.astype(bf)
+        for t in range(block_rows // tok):
+            index = first_row // tok + t
+            heads_out[index] = total[t * tok : (t + 1) * tok]
+
+            @pl.when(index != me)
+            def _():
+                remote(
+                    heads_out.at[index], token_in.at[me], so.at[index], ro.at[me], index
+                ).start()
+
+    token_in[me] = heads_out[me]
+    load.wait()
+    for j in range(1, n_sp):
+        other = (me + j) % n_sp
+        remote(
+            heads_out.at[other], token_in.at[other], so.at[other], ro.at[other], other
+        ).wait()
+    wide = heads * value_width
+    square = None
+    for s in range(n_sp):
+        piece = token_in[s].astype(jnp.float32)
+        part = jnp.sum(piece * piece, axis=-1, keepdims=True)
+        square = part if square is None else square + part
+    scale = lax.rsqrt(square / (n_sp * wide) + eps)
+    for s in range(n_sp):
+        span = slice(s * wide, (s + 1) * wide)
+        mixed[:, span] = (token_in[s].astype(jnp.float32) * scale * mix_gain_ref[:, span]).astype(bf)
+    stream = residual_ref[...].astype(jnp.float32) + dot32(mixed[...], out_weight_ref[...])
+    stream_ref[...] = stream
+    scale = lax.rsqrt(jnp.mean(stream * stream, axis=-1, keepdims=True) + eps)
+    normed_ref[...] = (stream * scale * ffn_gain_ref[...]).astype(bf)
+    for copy in down + across + sent:
+        copy.wait_send()
+
+
+def attended(
+    residual,
+    query,
+    latent,
+    rope_key,
+    latent_gain,
+    query_gain,
+    key_gain,
+    key_weight,
+    value_weight,
+    mix_gain,
+    out_weight,
+    ffn_gain,
+    head_count,
+    nope,
+    value_width,
+):
+    n_sp = lax.axis_size("sp")
+    n_y = n_sp // GROUPS
+    me = lax.axis_index("sp")
+    tok, width = residual.shape
+    rope = rope_key.shape[1]
+    qk = nope + rope
+    lat = latent.shape[1]
+    heads = head_count // n_sp
+    length = n_sp * tok
+    half = rope // 2
+    bf = jnp.bfloat16
+    query_blocks = query.reshape(tok, n_sp, heads * qk).transpose(1, 0, 2)
+    strips = lat // rope
+    tail = rope_key.reshape(strips, tok // strips, rope).transpose(1, 0, 2).reshape(-1, lat)
+    packed = jnp.concatenate([latent, tail], axis=0)
+    phases = angles(0, length, rope)
+    cos, sin = jnp.cos(phases), jnp.sin(phases)
+    cos = jnp.concatenate([jnp.ones((length, nope), jnp.float32), cos, cos], axis=1)
+    sin = jnp.concatenate([jnp.zeros((length, nope), jnp.float32), -sin, sin], axis=1)
+
+    def swap(gain):
+        return jnp.concatenate([gain[:nope], gain[nope + half :], gain[nope : nope + half]])
+
+    key_own = lax.dynamic_slice_in_dim(key_weight, me * heads * nope, heads * nope, 1)
+    value_own = lax.dynamic_slice_in_dim(value_weight, me * heads * value_width, heads * value_width, 1)
+    vmem = pl.BlockSpec(memory_space=pltpu.VMEM)
+    dma = pltpu.SemaphoreType.DMA
+    wide = heads * value_width
+    return pl.pallas_call(
+        functools.partial(attention_kernel, n_sp, n_y, heads, nope, rope, value_width),
+        out_shape=(
+            jax.ShapeDtypeStruct((tok, width), jnp.float32),
+            jax.ShapeDtypeStruct((tok, width), bf),
+        ),
+        in_specs=[vmem] * 14 + [pl.BlockSpec(memory_space=pl.ANY)],
+        out_specs=(vmem, vmem),
+        scratch_shapes=[
+            pltpu.VMEM(out_weight.shape, bf),
+            pltpu.VMEM((n_sp, tok, heads * qk), bf),
+            pltpu.VMEM((n_sp,) + packed.shape, bf),
+            pltpu.VMEM((heads, length, qk), bf),
+            pltpu.VMEM((heads, length, qk), bf),
+            pltpu.VMEM((length, wide), bf),
+            pltpu.VMEM((n_sp, tok, wide), bf),
+            pltpu.VMEM((n_sp, tok, wide), bf),
+            pltpu.VMEM((tok, n_sp * wide), bf),
+            dma((1,)),
+            dma((n_sp,)),
+            dma((n_sp,)),
+            dma((GROUPS,)),
+            dma((GROUPS,)),
+            dma((GROUPS, n_y)),
+            dma((GROUPS, n_y)),
+            dma((n_sp,)),
+            dma((n_sp,)),
+        ],
+        compiler_params=pltpu.CompilerParams(
+            collective_id=1, has_side_effects=True, vmem_limit_bytes=48 * 1024 * 1024
+        ),
+    )(
+        query_blocks,
+        packed,
+        latent_gain[None],
+        query_gain[None],
+        swap(query_gain)[None],
+        key_gain[None],
+        swap(key_gain)[None],
+        cos,
+        sin,
+        key_own,
+        value_own,
+        residual,
+        mix_gain[None],
+        ffn_gain[None],
+        out_weight,
+    )
 
 
 def routed(normed, stream, choice, group_prob, share, gate, up, down, expert_total):
@@ -364,51 +636,29 @@
     up_weight,
     down_weight,
 ):
-    tok_rows = residual.shape[1]
-    model_width = residual.shape[2]
     rope_width = rope_key.shape[2]
     qk_width = query_gain.shape[0]
     nope_width = qk_width - rope_width
     head_count = query.shape[2] // qk_width
     value_width = value_weight.shape[1] // head_count
     seq_devices = lax.axis_size("sp")
-    offset = lax.axis_index("sp") * tok_rows
-    own_phases = angles(offset, tok_rows, rope_width)
-    raw_query = query[0].astype(jnp.float32).reshape(tok_rows, head_count, qk_width)
-    queries_tok = head_vectors(
-        raw_query[..., :nope_width], raw_query[..., nope_width:], query_gain, own_phases
+    stream, normed = attended(
+        residual[0],
+        query[0],
+        latent[0],
+        rope_key[0],
+        latent_gain,
+        query_gain,
+        key_gain,
+        key_weight,
+        value_weight,
+        mix_gain,
+        out_weight,
+        ffn_gain,
+        head_count,
+        nope_width,
+        value_width,
     )
-    normed_latent = rms_scale(latent[0].astype(jnp.float32), latent_gain).astype(jnp.bfloat16)
-    key_part = jnp.dot(normed_latent, key_weight, preferred_element_type=jnp.float32).astype(
-        jnp.bfloat16
-    )
-    values_tok = jnp.dot(normed_latent, value_weight, preferred_element_type=jnp.float32).astype(
-        jnp.bfloat16
-    )
-    values_tok = values_tok.reshape(tok_rows, head_count, value_width)
-    shared_rope = jnp.broadcast_to(
-        rope_key[0].astype(jnp.float32)[:, None, :], (tok_rows, head_count, rope_width)
-    )
-    keys_tok = head_vectors(
-        key_part.astype(jnp.float32).reshape(tok_rows, head_count, nope_width),
-        shared_rope,
-        key_gain,
-        own_phases,
-    )
-    queries_head, keys_head, values_head = (
-        lax.all_to_all(queries_tok, "sp", split_axis=1, concat_axis=0, tiled=True),
-        lax.all_to_all(keys_tok, "sp", split_axis=1, concat_axis=0, tiled=True),
-        lax.all_to_all(values_tok, "sp", split_axis=1, concat_axis=0, tiled=True),
-    )
-    head_out = attend(queries_head, keys_head, values_head)
-    token_out = lax.all_to_all(head_out, "sp", split_axis=0, concat_axis=1, tiled=True).reshape(
-        tok_rows, head_count * value_width
-    )
-    mixed_in = rms_scale(token_out.astype(jnp.float32), mix_gain).astype(jnp.bfloat16)
-    stream = residual[0].astype(jnp.float32) + jnp.dot(
-        mixed_in, out_weight, preferred_element_type=jnp.float32
-    )
-    normed = rms_scale(stream, ffn_gain).astype(jnp.bfloat16)
     expert_total = seq_devices * lax.axis_size("dp")
     return routed(
         normed,

time: 159 us -> 130 us (0.82)
  Pallas kernels: 80.6 us -> 119 us
  waiting for transfers between devices: 30.3 us -> 0 us
  starting transfers between devices: 18.3 us -> 0 us
  matrix products: 8.33 us -> 0 us
  local copies, waits for them, and re-layouts: 12.1 us -> 6.77 us
  other arithmetic: 8.39 us -> 4.13 us
    pallas_call x0 -> x1, Pallas kernels: none -> 35.4 us  [attended(): pl.pallas_call(functools.partial(attention_kernel, n_sp, n_y, heads, nope...]
    all_to_all x4 -> x0, waiting for transfers between devices: 30.3 us -> none  [the longest x1 10.3 us: per_device(): lax.all_to_all(keys_tok, 'sp', split_axis=1, concat_axis=0, tiled=True)]
    all_to_all x4 -> x0, starting transfers between devices: 18.3 us -> none  [the longest x1 7.45 us: per_device(): lax.all_to_all(values_tok, 'sp', split_axis=1, concat_axis=0, tiled=True)]
    dot_general x11 -> x0, matrix products: 8.33 us -> none  [the longest x1 3.02 us: per_device(): jnp.dot(mixed_in, out_weight, preferred_element_type=jnp.float32)]
    reduce_sum x9 -> x0, other arithmetic: 2.76 us -> none  [the longest x4 1.48 us: attend(): row_sum = jnp.sum(raised, axis=-1)]
    pallas_call x1, Pallas kernels: 80.6 us -> 83.2 us  [routed(): pl.pallas_call(functools.partial(expert_kernel, n_y, n_dp, cap, rows), ou...]
    all_to_all x6 -> x0, local copies, waits for them, and re-layouts: 2.06 us -> none  [the longest x2 0.98 us: per_device(): lax.all_to_all(values_tok, 'sp', split_axis=1, concat_axis=0, tiled=True)]
    neg x0 -> x1, other arithmetic: none -> 1.9 us  [attended(): -sin]
  transfers between devices with their start and end apart: 4 -> 0, of which waited for: 4 -> 0; matrix products, arithmetic and copies ran while one was open for 6% -> 0% of each run, Pallas kernels for 0% -> 0%
where the time goes in v2:
time: 130 us
  Pallas kernels  119 us (92%)
  local copies, waits for them, and re-layouts  6.77 us (5%)
  other arithmetic  4.13 us (3%)
    pallas_call x1, Pallas kernels, routed(): pl.pallas_call(functools.partial(expert_kernel, n_y, n_dp, cap, rows), ou...  83.2 us
    pallas_call x1, Pallas kernels, attended(): pl.pallas_call(functools.partial(attention_kernel, n_sp, n_y, heads, nope...  35.4 us
    unnamed x33, local copies, waits for them, and re-layouts  4.28 us

profile of v2, /device:TPU:0, one launch (start us, length us, event | category | flops | bytes accessed | tf_op | source)
XLA Modules:
  0.0 129.8 jit_solution(17495788861166698607)
XLA Ops:
  0.0 0.0 copy-start.5
  0.0 0.0 copy-start.4
  0.0 0.0 copy-start.8
  0.0 1.9 %fusion = (f32[1024,16]{1,0:T(8,128)S(1)}, f32[1024,16]{1,0:T(8,128)S(1)}, f32[1024,16]{1,0:T(8,128)S(1)}) fusion(f32[16]{0:T(128)S(1)} %multiply_power_fusion, f32[1024]{0:T(1024)S(1)} %iota_convert_fusion), kind=kLoop, calls=%fused_computation.5 | loop fusion | flops 32768 | bytes 200768 | tf_op jit(solution)/shard_map/neg | solution.py:484
  2.0 0.0 copy-start.10
  2.0 0.0 copy-start.9
  2.0 0.0 copy-start.1
  2.0 0.0 copy-start.3
  2.0 0.0 copy-start.6
  2.1 0.0 copy-start.7
  2.1 0.6 pad_maximum_fusion
  2.7 0.9 constant_dynamic-slice_fusion
  3.6 0.0 copy-done.5
  3.6 0.1 fusion.8
  3.7 0.0 copy-done.4
  3.7 0.1 fusion.9
  3.7 0.1 maximum_bitcast_fusion
  3.8 0.0 copy-done.8
  3.8 0.2 copy.38
  4.1 0.2 copy.39
  4.3 0.0 copy-done.10
  4.3 0.1 copy.40
  4.4 0.1 reshape.85
  4.5 0.0 copy-done.9
  4.5 0.0 copy-done.1
  4.6 0.0 copy-done.3
  4.6 0.0 copy-done.6
  4.6 0.0 copy-done.7
  4.6 0.0 copy-start.12
  4.6 0.0 copy-start.11
  4.6 0.0 copy-start.13
  4.6 35.4 %shard_map.172 = (f32[128,2048]{1,0:T(8,128)S(1)}, bf16[128,2048]{1,0:T(8,128)(2,1)S(1)}) custom-call(bf16[8,128,192]{2,1,0:T(8,128)(2,1)S(1)} %bitcast.33, bf16[144,256]{1,0:T(8,128)(2,1)S(1)} %pad_maximum_fusion.2.packed_ref, f32[1,256]{1,0:T(1,128)S(1)} %bitcast.41, f32[1,96]{1,0:T(1,128)S(1)} %bitcast.37, f32[1,96]{1,0:T(1,128)S(1)} %get-tuple-element.29.query_swap_ref, ...), custom_call_target="tpu_custom_call" | custom-call | tf_op jit(solution)/shard_map/pallas_call | solution.py:494
  40.0 0.0 copy-start
  40.0 1.0 copy-done
  41.0 0.0 copy-start.2
  41.0 0.8 copy-done.2
  41.8 0.0 copy-done.12
  41.8 0.1 copy.43
  41.9 0.2 fusion.5
  42.1 0.1 subtract_multiply_fusion
  42.2 0.1 copy.47
  42.2 0.1 copy.45
  42.3 0.2 convert_reduce_fusion
  42.5 0.1 copy.49
  42.7 0.0 copy-done.11
  42.7 0.1 copy.48
  42.8 0.0 copy-done.13
  42.8 0.1 fusion.1
  42.9 0.1 fusion.6
  43.0 0.7 concatenate.24.info_ref
  43.8 0.2 convert_reduce_fusion.1
  44.0 0.7 compare_convert_fusion.pick_ref
  44.7 83.2 %shard_map.173 = bf16[128,2048]{1,0:T(8,128)(2,1)} custom-call(bf16[128,2048]{1,0:T(8,128)(2,1)} %copy-done.2, bf16[128,128]{1,0:T(8,128)(2,1)} %concatenate.24.info_ref, bf16[4,64,128]{2,1,0:T(8,128)(2,1)} %compare_convert_fusion.pick_ref, f32[128,2048]{1,0:T(8,128)} %copy-done, bf16[2048,512]{1,0:T(8,128)(2,1)} %bitcast.43, bf16[2048,512]{1,0:T(8,128)(2,1)} %bitcast.44, ...), custom_call_target="tpu_custom_call" | custom-call | tf_op jit(solution)/shard_map/pallas_call | solution.py:584
  127.9 1.9 %copy.51 = bf16[1,128,2048]{2,1,0:T(8,128)(2,1)} copy(bf16[1,128,2048]{2,1,0:T(8,128)(2,1)} %bitcast.42) | data formatting | bytes 1048576
  (15 shorter events, 0.1 us)
Async XLA Ops:
  0.0 3.6 %copy-start.5 = (f32[96]{0:T(128)S(1)}, f32[96]{0:T(128)}, u32[]{:S(2)}) copy-start(f32[96]{0:T(128)} %param.24) | copy-start | bytes 1156
  0.0 3.6 %copy-start.4 = (f32[96]{0:T(128)S(1)}, f32[96]{0:T(128)}, u32[]{:S(2)}) copy-start(f32[96]{0:T(128)} %param.23) | copy-start | bytes 1156
  0.0 3.8 %copy-start.8 = (bf16[1,128,1536]{2,1,0:T(8,128)(2,1)S(1)}, bf16[1,128,1536]{2,1,0:T(8,128)(2,1)}, u32[]{:S(2)}) copy-start(bf16[1,128,1536]{2,1,0:T(8,128)(2,1)} %param.19) | copy-start | bytes 1179652
  2.0 2.3 %copy-start.10 = (bf16[1,128,32]{1,2,0:T(8,128)(2,1)S(1)}, bf16[1,128,32]{1,2,0:T(8,128)(2,1)}, u32[]{:S(2)}) copy-start(bf16[1,128,32]{1,2,0:T(8,128)(2,1)} %param.21) | copy-start | bytes 24580
  2.0 2.5 %copy-start.9 = (bf16[1,128,256]{2,1,0:T(8,128)(2,1)S(1)}, bf16[1,128,256]{2,1,0:T(8,128)(2,1)}, u32[]{:S(2)}) copy-start(bf16[1,128,256]{2,1,0:T(8,128)(2,1)} %param.20) | copy-start | bytes 196612
  2.0 2.5 %copy-start.1 = (bf16[1,128,2048]{2,1,0:T(8,128)(2,1)S(1)}, bf16[1,128,2048]{2,1,0:T(8,128)(2,1)}, u32[]{:S(2)}) copy-start(bf16[1,128,2048]{2,1,0:T(8,128)(2,1)} %param.18) | copy-start | bytes 1572868
  2.0 2.5 %copy-start.3 = (f32[2048]{0:T(1024)S(1)}, f32[2048]{0:T(1024)}, u32[]{:S(2)}) copy-start(f32[2048]{0:T(1024)} %param.29) | copy-start | bytes 24580
  2.0 2.5 %copy-start.6 = (f32[1024]{0:T(1024)S(1)}, f32[1024]{0:T(1024)}, u32[]{:S(2)}) copy-start(f32[1024]{0:T(1024)} %param.27) | copy-start | bytes 12292
  2.1 2.5 %copy-start.7 = (f32[256]{0:T(256)S(1)}, f32[256]{0:T(256)}, u32[]{:S(2)}) copy-start(f32[256]{0:T(256)} %param.22) | copy-start | bytes 3076
  4.6 37.2 %copy-start.12 = (s32[1,128,2]{1,2,0:T(2,128)S(1)}, s32[1,128,2]{1,2,0:T(2,128)}, u32[]{:S(2)}) copy-start(s32[1,128,2]{1,2,0:T(2,128)} %param.30) | copy-start | bytes 3076
  4.6 38.1 %copy-start.11 = (f32[1,128,2]{1,2,0:T(2,128)S(1)}, f32[1,128,2]{1,2,0:T(2,128)}, u32[]{:S(2)}) copy-start(f32[1,128,2]{1,2,0:T(2,128)} %param.32) | copy-start | bytes 3076
  4.6 38.2 %copy-start.13 = (f32[1,128]{1,0:T(1,128)S(1)}, f32[1,128]{1,0:T(1,128)}, u32[]{:S(2)}) copy-start(f32[1,128]{1,0:T(1,128)} %param.31) | copy-start | bytes 1540
  40.0 1.0 copy-start
  41.0 0.8 copy-start.2

commit v3 on v2

--- a/solution.py
+++ b/solution.py
@@ -147,7 +147,7 @@
     def serve(k):
         for copy in second[k]:
             copy.wait_recv()
-        if k == 0:
+        if k == 2:
             for load in loads:
                 load.wait()
         given = arrive[k].reshape(peers * cap, width)
@@ -185,18 +185,18 @@
             acc[...] = stream_ref[...] + dot_t(pick_ref[plane], total.astype(jnp.bfloat16))
 
     scatter(0)
+    scatter(2)
     scatter(1)
+    scatter(3)
+    serve(2)
+    serve(1)
+    serve(3)
+    merge(2)
+    merge(1)
+    merge(3)
     serve(0)
-    scatter(3)
     merge(0)
-    serve(1)
-    scatter(2)
-    merge(1)
-    serve(3)
-    serve(2)
-    merge(3)
-    merge(2)
-    for k in (1, 3, 2):
+    for k in (2, 1, 3):
         fourth[k].wait_recv()
         acc[...] += dot_t(pick_ref[(plane + k) % GROUPS], home[k])
     out_ref[...] = acc[...].astype(jnp.bfloat16)

time: 130 us -> 122 us (0.938); the launches traced: 130 us -> 120 us
  Pallas kernels: 119 us -> 109 us
    pallas_call x1, Pallas kernels: 83.2 us -> 73.8 us  [routed(): pl.pallas_call(functools.partial(expert_kernel, n_y, n_dp, cap, rows), ou...]
where the time goes in v3:
time: 122 us; the launch traced here: 120 us
  Pallas kernels  109 us (89%)
  local copies, waits for them, and re-layouts  6.77 us (6%)
  other arithmetic  4.13 us (3%)
    pallas_call x1, Pallas kernels, routed(): pl.pallas_call(functools.partial(expert_kernel, n_y, n_dp, cap, rows), ou...  73.8 us
    pallas_call x1, Pallas kernels, attended(): pl.pallas_call(functools.partial(attention_kernel, n_sp, n_y, heads, nope...  35.4 us
    unnamed x33, local copies, waits for them, and re-layouts  4.28 us

profile of v3, /device:TPU:0, one launch (start us, length us, event | category | flops | bytes accessed | tf_op | source)
XLA Modules:
  0.0 120.4 jit_solution(17371675878835992024)
XLA Ops:
  0.0 0.0 copy-start.5
  0.0 0.0 copy-start.4
  0.0 0.0 copy-start.8
  0.0 1.9 %fusion = (f32[1024,16]{1,0:T(8,128)S(1)}, f32[1024,16]{1,0:T(8,128)S(1)}, f32[1024,16]{1,0:T(8,128)S(1)}) fusion(f32[16]{0:T(128)S(1)} %multiply_power_fusion, f32[1024]{0:T(1024)S(1)} %iota_convert_fusion), kind=kLoop, calls=%fused_computation.5 | loop fusion | flops 32768 | bytes 200768 | tf_op jit(solution)/shard_map/neg | solution.py:484
  2.0 0.0 copy-start.10
  2.0 0.0 copy-start.9
  2.0 0.0 copy-start.1
  2.0 0.0 copy-start.3
  2.0 0.0 copy-start.6
  2.1 0.0 copy-start.7
  2.1 0.6 pad_maximum_fusion
  2.7 0.9 constant_dynamic-slice_fusion
  3.6 0.0 copy-done.5
  3.6 0.1 fusion.8
  3.7 0.0 copy-done.4
  3.7 0.1 fusion.9
  3.7 0.1 maximum_bitcast_fusion
  3.8 0.0 copy-done.8
  3.8 0.2 copy.38
  4.1 0.2 copy.39
  4.3 0.0 copy-done.10
  4.3 0.1 copy.40
  4.4 0.1 reshape.85
  4.5 0.0 copy-done.9
  4.5 0.0 copy-done.1
  4.6 0.0 copy-done.3
  4.6 0.0 copy-done.6
  4.6 0.0 copy-done.7
  4.6 0.0 copy-start.12
  4.6 0.0 copy-start.11
  4.6 0.0 copy-start.13
  4.6 35.4 %shard_map.172 = (f32[128,2048]{1,0:T(8,128)S(1)}, bf16[128,2048]{1,0:T(8,128)(2,1)S(1)}) custom-call(bf16[8,128,192]{2,1,0:T(8,128)(2,1)S(1)} %bitcast.33, bf16[144,256]{1,0:T(8,128)(2,1)S(1)} %pad_maximum_fusion.2.packed_ref, f32[1,256]{1,0:T(1,128)S(1)} %bitcast.41, f32[1,96]{1,0:T(1,128)S(1)} %bitcast.37, f32[1,96]{1,0:T(1,128)S(1)} %get-tuple-element.29.query_swap_ref, ...), custom_call_target="tpu_custom_call" | custom-call | tf_op jit(solution)/shard_map/pallas_call | solution.py:494
  40.0 0.0 copy-start
  40.0 1.0 copy-done
  41.0 0.0 copy-start.2
  41.0 0.8 copy-done.2
  41.8 0.0 copy-done.12
  41.8 0.1 copy.43
  41.9 0.2 fusion.5
  42.1 0.1 subtract_multiply_fusion
  42.2 0.1 copy.47
  42.2 0.1 copy.45
  42.3 0.2 convert_reduce_fusion
  42.5 0.1 copy.49
  42.7 0.0 copy-done.11
  42.7 0.1 copy.48
  42.8 0.0 copy-done.13
  42.8 0.1 fusion.1
  42.9 0.1 fusion.6
  43.0 0.7 concatenate.24.info_ref
  43.8 0.2 convert_reduce_fusion.1
  44.0 0.7 compare_convert_fusion.pick_ref
  44.7 73.8 %shard_map.173 = bf16[128,2048]{1,0:T(8,128)(2,1)} custom-call(bf16[128,2048]{1,0:T(8,128)(2,1)} %copy-done.2, bf16[128,128]{1,0:T(8,128)(2,1)} %concatenate.24.info_ref, bf16[4,64,128]{2,1,0:T(8,128)(2,1)} %compare_convert_fusion.pick_ref, f32[128,2048]{1,0:T(8,128)} %copy-done, bf16[2048,512]{1,0:T(8,128)(2,1)} %bitcast.43, bf16[2048,512]{1,0:T(8,128)(2,1)} %bitcast.44, ...), custom_call_target="tpu_custom_call" | custom-call | tf_op jit(solution)/shard_map/pallas_call | solution.py:584
  118.5 1.9 %copy.51 = bf16[1,128,2048]{2,1,0:T(8,128)(2,1)} copy(bf16[1,128,2048]{2,1,0:T(8,128)(2,1)} %bitcast.42) | data formatting | bytes 1048576
  (15 shorter events, 0.1 us)
Async XLA Ops:
  0.0 3.6 %copy-start.5 = (f32[96]{0:T(128)S(1)}, f32[96]{0:T(128)}, u32[]{:S(2)}) copy-start(f32[96]{0:T(128)} %param.24) | copy-start | bytes 1156
  0.0 3.6 %copy-start.4 = (f32[96]{0:T(128)S(1)}, f32[96]{0:T(128)}, u32[]{:S(2)}) copy-start(f32[96]{0:T(128)} %param.23) | copy-start | bytes 1156
  0.0 3.8 %copy-start.8 = (bf16[1,128,1536]{2,1,0:T(8,128)(2,1)S(1)}, bf16[1,128,1536]{2,1,0:T(8,128)(2,1)}, u32[]{:S(2)}) copy-start(bf16[1,128,1536]{2,1,0:T(8,128)(2,1)} %param.19) | copy-start | bytes 1179652
  2.0 2.3 %copy-start.10 = (bf16[1,128,32]{1,2,0:T(8,128)(2,1)S(1)}, bf16[1,128,32]{1,2,0:T(8,128)(2,1)}, u32[]{:S(2)}) copy-start(bf16[1,128,32]{1,2,0:T(8,128)(2,1)} %param.21) | copy-start | bytes 24580
  2.0 2.5 %copy-start.9 = (bf16[1,128,256]{2,1,0:T(8,128)(2,1)S(1)}, bf16[1,128,256]{2,1,0:T(8,128)(2,1)}, u32[]{:S(2)}) copy-start(bf16[1,128,256]{2,1,0:T(8,128)(2,1)} %param.20) | copy-start | bytes 196612
  2.0 2.5 %copy-start.1 = (bf16[1,128,2048]{2,1,0:T(8,128)(2,1)S(1)}, bf16[1,128,2048]{2,1,0:T(8,128)(2,1)}, u32[]{:S(2)}) copy-start(bf16[1,128,2048]{2,1,0:T(8,128)(2,1)} %param.18) | copy-start | bytes 1572868
  2.0 2.5 %copy-start.3 = (f32[2048]{0:T(1024)S(1)}, f32[2048]{0:T(1024)}, u32[]{:S(2)}) copy-start(f32[2048]{0:T(1024)} %param.29) | copy-start | bytes 24580
  2.0 2.5 %copy-start.6 = (f32[1024]{0:T(1024)S(1)}, f32[1024]{0:T(1024)}, u32[]{:S(2)}) copy-start(f32[1024]{0:T(1024)} %param.27) | copy-start | bytes 12292
  2.1 2.5 %copy-start.7 = (f32[256]{0:T(256)S(1)}, f32[256]{0:T(256)}, u32[]{:S(2)}) copy-start(f32[256]{0:T(256)} %param.22) | copy-start | bytes 3076
  4.6 37.2 %copy-start.12 = (s32[1,128,2]{1,2,0:T(2,128)S(1)}, s32[1,128,2]{1,2,0:T(2,128)}, u32[]{:S(2)}) copy-start(s32[1,128,2]{1,2,0:T(2,128)} %param.30) | copy-start | bytes 3076
  4.6 38.1 %copy-start.11 = (f32[1,128,2]{1,2,0:T(2,128)S(1)}, f32[1,128,2]{1,2,0:T(2,128)}, u32[]{:S(2)}) copy-start(f32[1,128,2]{1,2,0:T(2,128)} %param.32) | copy-start | bytes 3076
  4.6 38.2 %copy-start.13 = (f32[1,128]{1,0:T(1,128)S(1)}, f32[1,128]{1,0:T(1,128)}, u32[]{:S(2)}) copy-start(f32[1,128]{1,0:T(1,128)} %param.31) | copy-start | bytes 1540
  40.0 1.0 copy-start
  41.0 0.8 copy-start.2
